TPU v7x, 32 devices: a whole 2x2x4 slice. The times are simulated.
32 devices in a mesh: ep: 8 (over z, core), tp: 4 (over y, x).
Axes of the slice: x: 2, y: 2, z: 4, core: 2. Of those that a mesh axis runs over, the one named last changes fastest.
Arguments:
- tokens: bfloat16 [1024, 2048], P('ep', 'tp'), may hold values from -3000 to 3000
- norm_gain: float32 [2048], replicated, may hold values from 0.1 to 1.9
- gate_weight: bfloat16 [8, 2048, 512], P('ep'), may hold values from -0.125 to 0.125
- up_weight: bfloat16 [8, 2048, 512], P('ep'), may hold values from -0.125 to 0.125
- down_weight: bfloat16 [8, 512, 2048], P('ep'), may hold values from -0.25 to 0.25
- expert_ids: int32 [1024, 2], P('ep'), may hold values from 0 to 7, as said below
- route_weight: float32 [1024, 2], P('ep'), may hold values from 0.2 to 1
Outputs:
- mixed: bfloat16 [1024, 2048], P('ep', 'tp')
Inputs may be any that keep to these rules, and one draw needn't show every extreme that they name: `expert_ids`: A token's two experts differ and lie in one group of 2 consecutive experts. In each aligned block of 32 rows no expert is named more than 16 times, and in every block all experts of one group, the same group for all blocks, are named exactly 16 times.
All inputs are finite; a program needn't handle non-finite values.
Results may differ from a plain program's by a relative error of at most 0.0071.
Values may be sent and summed in bfloat16 or wider, within the bound.
A program may use at most 64 MiB of HBM per device.

v0:
```python
import math
from functools import partial

import jax
import jax.numpy as jnp
from jax import lax
from jax.experimental import pallas as pl
from jax.experimental.pallas import tpu as pltpu
from jax.sharding import PartitionSpec as P


def slot_numbers(block_ids, experts):
    flat_ids = block_ids.reshape(-1)
    hit_table = (flat_ids[:, None] == jnp.arange(experts, dtype=jnp.int32)[None, :]).astype(
        jnp.int32
    )
    earlier = jnp.cumsum(hit_table, axis=0) - hit_table
    return (flat_ids, jnp.sum(earlier * hit_table, axis=1))


def placement_matrix(flat_ids, slot_index, experts, capacity):
    target = (flat_ids * capacity + slot_index).reshape(-1, 2)
    slot_rows = jnp.arange(experts * capacity, dtype=jnp.int32)[:, None]
    first_hit = (target[:, 0][None, :] == slot_rows).astype(jnp.bfloat16)
    second_hit = (target[:, 1][None, :] == slot_rows).astype(jnp.bfloat16)
    return first_hit + second_hit


def expert_apply(row_data, gate_weight, up_weight, down_weight):
    shape_in = row_data.shape
    flat_rows = row_data.reshape(-1, shape_in[-1])
    gate_part = jnp.dot(flat_rows, gate_weight[0], preferred_element_type=jnp.float32)
    up_part = jnp.dot(flat_rows, up_weight[0], preferred_element_type=jnp.float32)
    hidden = (jax.nn.silu(gate_part) * up_part).astype(jnp.bfloat16)
    produced = jnp.dot(hidden, down_weight[0], preferred_element_type=jnp.float32).astype(
        jnp.bfloat16
    )
    return produced.reshape(shape_in[:-1] + (produced.shape[-1],))


def local(tokens, norm_gain, gate_weight, up_weight, down_weight, expert_ids, route_weight):
    tp_count = lax.axis_size("tp")
    experts = lax.axis_size("ep") * gate_weight.shape[0]
    model_width = gate_weight.shape[1]
    group_rows = tokens.shape[0]
    block_rows = group_rows // tp_count
    capacity = 4 * block_rows // experts
    tp_index = lax.axis_index("tp")
    apply_experts = partial(
        expert_apply, gate_weight=gate_weight, up_weight=up_weight, down_weight=down_weight
    )
    full_rows = lax.all_to_all(tokens, "tp", split_axis=0, concat_axis=1, tiled=True)
    block_ids = lax.dynamic_slice_in_dim(expert_ids, tp_index * block_rows, block_rows, 0)
    block_weight = lax.dynamic_slice_in_dim(route_weight, tp_index * block_rows, block_rows, 0)
    widened = full_rows.astype(jnp.float32)
    mean_square = jnp.mean(widened * widened, axis=-1, keepdims=True)
    normed = (widened * lax.rsqrt(mean_square + 1e-06) * norm_gain).astype(jnp.bfloat16)
    flat_ids, slot_index = slot_numbers(block_ids, experts)
    placing = placement_matrix(flat_ids, slot_index, experts, capacity)
    outgoing = jnp.dot(placing, normed, preferred_element_type=jnp.float32).astype(jnp.bfloat16)
    outgoing = outgoing.reshape(experts, capacity, model_width)
    produced = apply_experts(
        lax.all_to_all(outgoing, "ep", split_axis=0, concat_axis=0, tiled=True)
    )
    returned = lax.all_to_all(produced, "ep", split_axis=0, concat_axis=0, tiled=True)
    picked = jnp.take(returned.reshape(-1, model_width), flat_ids * capacity + slot_index, axis=0)
    weighted = picked.astype(jnp.float32) * block_weight.reshape(-1)[:, None]
    mixed_rows = weighted.reshape(block_rows, 2, model_width).sum(axis=1).astype(jnp.bfloat16)
    return lax.all_to_all(mixed_rows, "tp", split_axis=1, concat_axis=0, tiled=True)


def direct_kernel(
    dims,
    ids_hbm,
    mix_hbm,
    tok_hbm,
    gain_hbm,
    gate_hbm,
    up_hbm,
    down_hbm,
    out_ref,
    ids_ref,
    mix_ref,
    tok_ref,
    gain_ref,
    pick_buf,
    send_buf,
    weight_send,
    row_buf,
    weight_buf,
    gate_buf,
    up_buf,
    down_own,
    down_other,
    hidden_own,
    hidden_other,
    result_buf,
    back_buf,
    load_sem,
    row_send_sem,
    row_recv_sem,
    weight_send_sem,
    weight_recv_sem,
    pass_send_sem,
    pass_recv_sem,
    pair_send_sem,
    pair_recv_sem,
    back_send_sem,
    back_recv_sem,
):
    ep_count, tp_count, group, cap = dims
    chips = ep_count // group
    rows, width = tok_ref.shape
    block_rows = rows // tp_count
    half_cols = down_own.shape[1]
    half_tp = tp_count // group
    ep_me = lax.axis_index("ep")
    tp_me = lax.axis_index("tp")
    chip_me = ep_me // group
    core_me = ep_me % group
    core_other = 1 - core_me
    partner = (chip_me * group + core_other, tp_me)

    def slot_at(chip, block):
        return pl.ds(pl.multiple_of((chip * tp_count + block) * cap, cap), cap)

    def chip_at(step):
        chip, bit = 0, 1
        while bit < chips:
            chip, bit = chip + (chip_me // bit + step // bit) % 2 * bit, 2 * bit
        return chip

    order = [
        half * chips // 2 + offset
        for offset in range(chips // 2)
        for half in (1, 0)
    ]
    phases = chips // 2
    per_phase = chips // phases
    phase_rows = per_phase * group * cap

    def rows_at(step, core):
        return pl.ds(pl.multiple_of((order.index(step) * group + core) * cap, cap), cap)

    def cols_at(index):
        return pl.ds(pl.multiple_of(index * width, width), width)

    def half_at(core):
        return pl.ds(pl.multiple_of(core * half_cols, half_cols), half_cols)

    def remote(src, dst, send_sem, recv_sem, target):
        return pltpu.make_async_remote_copy(
            src_ref=src,
            dst_ref=dst,
            send_sem=send_sem,
            recv_sem=recv_sem,
            device_id=target,
            device_id_type=pl.DeviceIdType.MESH,
        )

    small_loads = [
        pltpu.make_async_copy(ids_hbm, ids_ref, load_sem.at[3]),
        pltpu.make_async_copy(mix_hbm, mix_ref, load_sem.at[4]),
        pltpu.make_async_copy(tok_hbm, tok_ref, load_sem.at[5]),
        pltpu.make_async_copy(gain_hbm, gain_ref, load_sem.at[6]),
    ]
    loads = [
        pltpu.make_async_copy(gate_hbm.at[0], gate_buf, load_sem.at[0]),
        pltpu.make_async_copy(up_hbm.at[0], up_buf, load_sem.at[1]),
        pltpu.make_async_copy(down_hbm.at[0, :, half_at(core_me)], down_own, load_sem.at[2]),
    ]
    for load in small_loads + loads:
        load.start()

    barrier = pltpu.get_barrier_semaphore()
    for step_ep in range(ep_count):
        for step_tp in range(tp_count):
            if step_ep or step_tp:
                pl.semaphore_signal(
                    barrier,
                    inc=1,
                    device_id=(
                        (ep_me + step_ep) % ep_count,
                        (tp_me + step_tp) % tp_count,
                    ),
                    device_id_type=pl.DeviceIdType.MESH,
                )

    row_of = lax.broadcasted_iota(jnp.int32, (rows, rows), 0)
    col_of = lax.broadcasted_iota(jnp.int32, (rows, rows), 1)

    def upright(line):
        return jnp.sum(jnp.where(row_of == col_of, line, 0.0), axis=1, keepdims=True)

    small_loads[0].wait()
    small_loads[1].wait()
    ids = ids_ref[...].astype(jnp.float32)
    mixes = mix_ref[...]
    first_id, second_id = upright(ids[0:1, :]), upright(ids[1:2, :])
    first_mix, second_mix = upright(mixes[0:1, :]), upright(mixes[1:2, :])
    group_of = jnp.zeros((rows, 1), jnp.float32)
    for chip in range(1, chips):
        group_of += (first_id >= chip * group).astype(jnp.float32)
    lanes = lax.broadcasted_iota(jnp.int32, (rows, 128), 1)
    shift = block_rows.bit_length() - 1
    earlier = (col_of < row_of) & ((col_of >> shift) == (row_of >> shift))
    member = (group_of == lanes.astype(jnp.float32)).astype(jnp.float32)
    counts = jnp.dot(
        earlier.astype(jnp.float32).astype(jnp.bfloat16),
        member.astype(jnp.bfloat16),
        preferred_element_type=jnp.float32,
    )
    rank = jnp.sum(counts * member, axis=1, keepdims=True)
    block_of = (lax.broadcasted_iota(jnp.int32, (rows, 1), 0) >> shift).astype(jnp.float32)
    target_slot = (group_of * tp_count + block_of) * cap + rank
    slots = chips * tp_count * cap
    slot_of = lax.broadcasted_iota(jnp.int32, (rows, slots), 1).astype(jnp.float32)
    pick = (slot_of == target_slot).astype(jnp.float32).astype(jnp.bfloat16)
    pick_buf[...] = pick
    across = (((0,), (0,)), ((), ()))
    small_loads[2].wait()
    send_buf[...] = lax.dot_general(
        pick, tok_ref[...], across, preferred_element_type=jnp.float32
    ).astype(jnp.bfloat16)
    in_order = first_id < second_id
    low_mix = jnp.where(in_order, first_mix, second_mix)
    high_mix = jnp.where(in_order, second_mix, first_mix)
    low_top = low_mix.astype(jnp.bfloat16).astype(jnp.float32)
    high_top = high_mix.astype(jnp.bfloat16).astype(jnp.float32)
    mix_cols = jnp.where(lanes == 0, low_top, 0.0)
    mix_cols = jnp.where(lanes == 1, high_top, mix_cols)
    mix_cols = jnp.where(lanes == 2, low_mix - low_top, mix_cols)
    mix_cols = jnp.where(lanes == 3, high_mix - high_top, mix_cols)
    weight_send[...] = lax.dot_general(
        pick, mix_cols.astype(jnp.bfloat16), across, preferred_element_type=jnp.float32
    ).astype(jnp.bfloat16)

    small_loads[3].wait()
    pl.semaphore_wait(barrier, ep_count * tp_count - 1)

    sends = []
    for step_chip in order:
        chip = chip_at(step_chip)
        src = weight_send.at[slot_at(chip, tp_me)]
        dst = weight_buf.at[rows_at(step_chip, core_me)]
        if step_chip == 0:
            pltpu.make_async_copy(src, dst, weight_recv_sem.at[step_chip]).start()
        else:
            copy = remote(
                src,
                dst,
                weight_send_sem.at[step_chip],
                weight_recv_sem.at[step_chip],
                (chip * group + core_me, tp_me),
            )
            copy.start()
            sends.append(copy)
        for step_tp in reversed(range(tp_count)):
            block = (tp_me + step_tp) % tp_count
            src = send_buf.at[slot_at(chip, block)]
            dst = row_buf.at[rows_at(step_chip, core_me), cols_at(tp_me)]
            if step_chip == 0 and step_tp == 0:
                pltpu.make_async_copy(src, dst, row_recv_sem.at[step_chip, tp_me]).start()
            else:
                copy = remote(
                    src,
                    dst,
                    row_send_sem.at[step_chip, step_tp],
                    row_recv_sem.at[step_chip, tp_me],
                    (chip * group + core_me, block),
                )
                copy.start()
                sends.append(copy)
    down_copy = remote(
        down_hbm.at[0, :, half_at(core_other)],
        down_other,
        pair_send_sem.at[phases],
        pair_recv_sem.at[phases],
        partner,
    )
    down_copy.start()

    def receive(phase):
        steps = order[phase * per_phase : (phase + 1) * per_phase]
        passes = []
        for step_chip in reversed(steps):
            for step_tp in range(tp_count):
                block = (tp_me + step_tp) % tp_count
                pltpu.make_async_copy(
                    send_buf.at[slot_at(chip_me, block)],
                    row_buf.at[rows_at(step_chip, core_me), cols_at(block)],
                    row_recv_sem.at[step_chip, block],
                ).wait()
            pltpu.make_async_copy(
                weight_send.at[slot_at(chip_me, tp_me)],
                weight_buf.at[rows_at(step_chip, core_me)],
                weight_recv_sem.at[step_chip],
            ).wait()
            for which, held_buf in enumerate((row_buf, weight_buf)):
                held = held_buf.at[rows_at(step_chip, core_me)]
                copy = remote(
                    held,
                    held,
                    pass_send_sem.at[which, step_chip],
                    pass_recv_sem.at[which, step_chip],
                    partner,
                )
                copy.start()
                passes.append(copy)
        return passes

    passes = receive(0)
    for phase in range(phases):
        steps = order[phase * per_phase : (phase + 1) * per_phase]
        for copy in passes:
            copy.wait_recv()
        sends += passes

        held = slice(phase * phase_rows, (phase + 1) * phase_rows)
        widened = row_buf[held, :].astype(jnp.float32)
        mean_square = jnp.mean(widened * widened, axis=-1, keepdims=True)
        normed = (widened * lax.rsqrt(mean_square + 1e-06) * gain_ref[...]).astype(jnp.bfloat16)
        if phase == 0:
            loads[0].wait()
        gate_part = jnp.dot(normed, gate_buf[...], preferred_element_type=jnp.float32)
        if phase == 0:
            loads[1].wait()
        up_part = jnp.dot(normed, up_buf[...], preferred_element_type=jnp.float32)
        mixes = weight_buf[held, :].astype(jnp.float32)
        low = mixes[:, 0:1] + mixes[:, 2:3]
        high = mixes[:, 1:2] + mixes[:, 3:4]
        mix = jnp.where(core_me == 0, low, high)
        hidden = (gate_part / (1.0 + jnp.exp(-gate_part)) * up_part * mix).astype(jnp.bfloat16)
        hidden_own[held, :] = hidden
        hidden_copy = remote(
            hidden_own.at[held],
            hidden_other.at[held],
            pair_send_sem.at[phase],
            pair_recv_sem.at[phase],
            partner,
        )
        hidden_copy.start()
        sends.append(hidden_copy)
        if phase + 1 < phases:
            passes = receive(phase + 1)
        if phase == 0:
            loads[2].wait()
        own_part = jnp.dot(hidden, down_own[...], preferred_element_type=jnp.float32)
        if phase == 0:
            down_copy.wait_recv()
        hidden_copy.wait_recv()
        other = hidden_other[held, :]
        for part in range(half_tp):
            part_cols = slice(part * width, (part + 1) * width)
            result_buf[held, part_cols] = (
                own_part[:, part_cols]
                + jnp.dot(other, down_other[:, part_cols], preferred_element_type=jnp.float32)
            ).astype(jnp.bfloat16)
            feature = core_me * half_tp + part
            for step_chip in steps:
                chip = chip_at(step_chip)
                for step_core in range(group):
                    core = (core_me + step_core) % group
                    src = result_buf.at[rows_at(step_chip, core), part_cols]
                    dst = back_buf.at[slot_at(chip_me, tp_me)]
                    copy = remote(
                        src,
                        dst,
                        back_send_sem.at[part, step_chip, step_core],
                        back_recv_sem.at[step_chip, tp_me],
                        (chip * group + core, feature),
                    )
                    if step_chip == 0 and step_core == 0:

                        @pl.when(feature == tp_me)
                        def _():
                            pltpu.make_async_copy(
                                src, dst, back_recv_sem.at[step_chip, tp_me]
                            ).start()

                        @pl.when(feature != tp_me)
                        def _():
                            copy.start()
                    else:
                        copy.start()
                        sends.append(copy)

    for step_chip in order:
        for step_tp in range(tp_count):
            block = (tp_me + step_tp) % tp_count
            pltpu.make_async_copy(
                result_buf.at[pl.ds(0, cap), pl.ds(0, width)],
                back_buf.at[slot_at(chip_at(step_chip), block)],
                back_recv_sem.at[step_chip, block],
            ).wait()
    out_ref[...] = jnp.dot(
        pick_buf[...], back_buf[...], preferred_element_type=jnp.float32
    ).astype(out_ref.dtype)

    for copy in sends + [down_copy]:
        copy.wait_send()
    for part in range(half_tp):
        feature = core_me * half_tp + part

        @pl.when(feature != tp_me)
        def _():
            remote(
                result_buf.at[pl.ds(0, cap), pl.ds(part * width, width)],
                back_buf.at[slot_at(chip_me, tp_me)],
                back_send_sem.at[part, 0, 0],
                back_recv_sem.at[0, tp_me],
                (ep_me, feature),
            ).wait_send()


def direct(tokens, norm_gain, gate_weight, up_weight, down_weight, expert_ids, route_weight):
    ep_count, tp_count = lax.axis_size("ep"), lax.axis_size("tp")
    group = math.isqrt(ep_count * gate_weight.shape[0])
    rows, width = tokens.shape
    cap = 4 * (rows // tp_count) // ep_count * group // 2
    chips = ep_count // group
    model_width, hidden_width = gate_weight.shape[1:]
    slots = chips * tp_count * cap
    held = ep_count * cap
    half_cols = model_width // group
    vmem, dma = pltpu.VMEM, pltpu.SemaphoreType.DMA
    low = jnp.bfloat16
    in_vmem = pl.BlockSpec(memory_space=pltpu.VMEM)
    in_hbm = pl.BlockSpec(memory_space=pltpu.HBM)
    return pl.pallas_call(
        partial(direct_kernel, (ep_count, tp_count, group, cap)),
        out_shape=jax.ShapeDtypeStruct((rows, width), low),
        in_specs=[in_hbm] * 7,
        out_specs=in_vmem,
        scratch_shapes=[
            vmem((2, rows), jnp.int32),
            vmem((2, rows), jnp.float32),
            vmem((rows, width), low),
            vmem((1, model_width), jnp.float32),
            vmem((rows, slots), low),
            vmem((slots, width), low),
            vmem((slots, 128), low),
            vmem((held, model_width), low),
            vmem((held, 128), low),
            vmem((model_width, hidden_width), low),
            vmem((model_width, hidden_width), low),
            vmem((hidden_width, half_cols), low),
            vmem((hidden_width, half_cols), low),
            vmem((held, hidden_width), low),
            vmem((held, hidden_width), low),
            vmem((held, half_cols), low),
            vmem((slots, width), low),
            dma((7,)),
            dma((chips, tp_count)),
            dma((chips, tp_count)),
            dma((chips,)),
            dma((chips,)),
            dma((2, chips)),
            dma((2, chips)),
            dma((chips // 2 + 1,)),
            dma((chips // 2 + 1,)),
            dma((tp_count // group, chips, group)),
            dma((chips, tp_count)),
        ],
        compiler_params=pltpu.CompilerParams(
            collective_id=0, has_side_effects=True, vmem_limit_bytes=67043328
        ),
    )(
        expert_ids.T,
        route_weight.T,
        tokens,
        norm_gain.reshape(1, -1),
        gate_weight,
        up_weight,
        down_weight,
    )


def layer(tokens, norm_gain, gate_weight, up_weight, down_weight, expert_ids, route_weight):
    group = math.isqrt(lax.axis_size("ep") * gate_weight.shape[0])
    body = direct if group == 2 and gate_weight.shape[0] == 1 else local
    return body(
        tokens, norm_gain, gate_weight, up_weight, down_weight, expert_ids, route_weight
    )


def solution(mesh):
    in_specs = (
        P("ep", "tp"),
        P(),
        P("ep", None, None),
        P("ep", None, None),
        P("ep", None, None),
        P("ep", None),
        P("ep", None),
    )
    out_specs = P("ep", "tp")
    return jax.shard_map(layer, mesh=mesh, in_specs=in_specs, out_specs=out_specs, check_vma=False)
```

profile of v0, /device:TPU:0, one launch (start us, length us, event | category | flops | bytes accessed | tf_op | source)
XLA Modules:
  0.0 26.9 jit_solution(4134324284667546698)
XLA Ops:
  0.0 25.3 %shard_map.73 = bf16[128,512]{1,0:T(8,128)(2,1)} custom-call(s32[2,128]{1,0:T(2,128)} %bitcast.4, f32[2,128]{1,0:T(2,128)} %bitcast.5, bf16[128,512]{1,0:T(8,128)(2,1)} %tok_hbm.1, f32[1,2048]{1,0:T(1,128)} %bitcast.3, bf16[1,2048,512]{2,1,0:T(8,128)(2,1)} %gate_hbm.1, bf16[1,2048,512]{2,1,0:T(8,128)(2,1)} %up_hbm.1, bf16[1,512,2048]{2,1,0:T(8,128)(2,1)} %down_hbm.1), custom_call_target="tpu_custom_call" | custom-call | tf_op jit(solution)/shard_map/pallas_call | solution.py:430
  25.3 1.6 %copy.9 = bf16[128,512]{1,0:T(8,128)(2,1)} copy(bf16[128,512]{1,0:T(8,128)(2,1)} %shard_map.73) | data formatting | bytes 262144
where the time goes:
time: 27.1 us; the launch traced here: 26.9 us
  Pallas kernels  25.3 us (93%)
  local copies, waits for them, and re-layouts  1.57 us (6%)
    pallas_call x1, Pallas kernels, direct(): pl.pallas_call(partial(direct_kernel, (ep_count, tp_count, group, cap)),...  25.3 us
    unnamed x1, local copies, waits for them, and re-layouts  1.57 us

commit v1 on v0

v1 whole, which is shorter than its diff:
```python
import math
from functools import partial

import jax
import jax.numpy as jnp
from jax import lax
from jax.experimental import pallas as pl
from jax.experimental.pallas import tpu as pltpu
from jax.sharding import PartitionSpec as P


def slot_numbers(block_ids, experts):
    flat_ids = block_ids.reshape(-1)
    hit_table = (flat_ids[:, None] == jnp.arange(experts, dtype=jnp.int32)[None, :]).astype(
        jnp.int32
    )
    earlier = jnp.cumsum(hit_table, axis=0) - hit_table
    return (flat_ids, jnp.sum(earlier * hit_table, axis=1))


def placement_matrix(flat_ids, slot_index, experts, capacity):
    target = (flat_ids * capacity + slot_index).reshape(-1, 2)
    slot_rows = jnp.arange(experts * capacity, dtype=jnp.int32)[:, None]
    first_hit = (target[:, 0][None, :] == slot_rows).astype(jnp.bfloat16)
    second_hit = (target[:, 1][None, :] == slot_rows).astype(jnp.bfloat16)
    return first_hit + second_hit


def expert_apply(row_data, gate_weight, up_weight, down_weight):
    shape_in = row_data.shape
    flat_rows = row_data.reshape(-1, shape_in[-1])
    gate_part = jnp.dot(flat_rows, gate_weight[0], preferred_element_type=jnp.float32)
    up_part = jnp.dot(flat_rows, up_weight[0], preferred_element_type=jnp.float32)
    hidden = (jax.nn.silu(gate_part) * up_part).astype(jnp.bfloat16)
    produced = jnp.dot(hidden, down_weight[0], preferred_element_type=jnp.float32).astype(
        jnp.bfloat16
    )
    return produced.reshape(shape_in[:-1] + (produced.shape[-1],))


def local(tokens, norm_gain, gate_weight, up_weight, down_weight, expert_ids, route_weight):
    tp_count = lax.axis_size("tp")
    experts = lax.axis_size("ep") * gate_weight.shape[0]
    model_width = gate_weight.shape[1]
    group_rows = tokens.shape[0]
    block_rows = group_rows // tp_count
    capacity = 4 * block_rows // experts
    tp_index = lax.axis_index("tp")
    apply_experts = partial(
        expert_apply, gate_weight=gate_weight, up_weight=up_weight, down_weight=down_weight
    )
    full_rows = lax.all_to_all(tokens, "tp", split_axis=0, concat_axis=1, tiled=True)
    block_ids = lax.dynamic_slice_in_dim(expert_ids, tp_index * block_rows, block_rows, 0)
    block_weight = lax.dynamic_slice_in_dim(route_weight, tp_index * block_rows, block_rows, 0)
    widened = full_rows.astype(jnp.float32)
    mean_square = jnp.mean(widened * widened, axis=-1, keepdims=True)
    normed = (widened * lax.rsqrt(mean_square + 1e-06) * norm_gain).astype(jnp.bfloat16)
    flat_ids, slot_index = slot_numbers(block_ids, experts)
    placing = placement_matrix(flat_ids, slot_index, experts, capacity)
    outgoing = jnp.dot(placing, normed, preferred_element_type=jnp.float32).astype(jnp.bfloat16)
    outgoing = outgoing.reshape(experts, capacity, model_width)
    produced = apply_experts(
        lax.all_to_all(outgoing, "ep", split_axis=0, concat_axis=0, tiled=True)
    )
    returned = lax.all_to_all(produced, "ep", split_axis=0, concat_axis=0, tiled=True)
    picked = jnp.take(returned.reshape(-1, model_width), flat_ids * capacity + slot_index, axis=0)
    weighted = picked.astype(jnp.float32) * block_weight.reshape(-1)[:, None]
    mixed_rows = weighted.reshape(block_rows, 2, model_width).sum(axis=1).astype(jnp.bfloat16)
    return lax.all_to_all(mixed_rows, "tp", split_axis=1, concat_axis=0, tiled=True)


def direct_kernel(
    dims,
    ids_hbm,
    mix_hbm,
    tok_hbm,
    gain_hbm,
    gate_hbm,
    up_hbm,
    down_hbm,
    out_ref,
    ids_ref,
    mix_ref,
    tok_ref,
    gain_ref,
    pick_buf,
    send_buf,
    weight_send,
    row_buf,
    wide_buf,
    down_buf,
    hidden_buf,
    result_buf,
    back_buf,
    load_sem,
    row_send_sem,
    row_recv_sem,
    weight_send_sem,
    pass_send_sem,
    pass_recv_sem,
    pair_send_sem,
    pair_recv_sem,
    down_send_sem,
    down_recv_sem,
    back_send_sem,
    back_recv_sem,
):
    ep_count, tp_count, group, cap = dims
    chips = ep_count // group
    rows, width = tok_ref.shape
    model_width = gain_ref.shape[1]
    hidden_width = gate_hbm.shape[2]
    block_rows = rows // tp_count
    half_cols = down_buf.shape[1]
    half_tp = tp_count // group
    ep_me = lax.axis_index("ep")
    tp_me = lax.axis_index("tp")
    chip_me = ep_me // group
    core_me = ep_me % group
    core_other = 1 - core_me
    partner = (chip_me * group + core_other, tp_me)
    send_table = ((2, 3, 1), (3, 2, 0), (0, 1, 3), (1, 0, 2))
    turn_table = ((0, 3, 2, 1), (1, 3, 2, 0), (2, 0, 1, 3), (3, 0, 1, 2))
    phase_rows = group * cap

    def slot_at(chip, block):
        return pl.ds(pl.multiple_of((chip * tp_count + block) * cap, cap), cap)

    def entry(table, row, column):
        picked = table[0][column]
        for other in range(1, chips):
            picked = jnp.where(row == other, table[other][column], picked)
        return picked

    def turn_at(here, there):
        turn = 0
        for late in range(1, chips):
            turn = jnp.where(entry(turn_table, here, late) == there, late, turn)
        return turn

    def rows_at(turn, core):
        return pl.ds(pl.multiple_of((turn * group + core) * cap, cap), cap)

    def held_at(turn):
        return pl.ds(pl.multiple_of(turn * phase_rows, phase_rows), phase_rows)

    def cols_at(index):
        return pl.ds(pl.multiple_of(index * width, width), width)

    def half_at(core):
        return pl.ds(pl.multiple_of(core * half_cols, half_cols), half_cols)

    def remote(src, dst, send_sem, recv_sem, target):
        return pltpu.make_async_remote_copy(
            src_ref=src,
            dst_ref=dst,
            send_sem=send_sem,
            recv_sem=recv_sem,
            device_id=target,
            device_id_type=pl.DeviceIdType.MESH,
        )

    def settle(ref, sem):
        pltpu.make_async_copy(ref, ref, sem).wait()

    small_loads = [
        pltpu.make_async_copy(ids_hbm, ids_ref, load_sem.at[2]),
        pltpu.make_async_copy(mix_hbm, mix_ref, load_sem.at[3]),
        pltpu.make_async_copy(tok_hbm, tok_ref, load_sem.at[4]),
        pltpu.make_async_copy(gain_hbm, gain_ref, load_sem.at[5]),
    ]
    gate_load = pltpu.make_async_copy(
        gate_hbm.at[0], wide_buf.at[:, pl.ds(0, hidden_width)], load_sem.at[0]
    )
    up_load = pltpu.make_async_copy(
        up_hbm.at[0], wide_buf.at[:, pl.ds(hidden_width, hidden_width)], load_sem.at[1]
    )
    down_load = pltpu.make_async_copy(
        down_hbm.at[0, :, half_at(core_me)],
        down_buf.at[pl.ds(0, hidden_width), :],
        load_sem.at[6],
    )
    for load in small_loads + [gate_load, up_load, down_load]:
        load.start()

    barrier = pltpu.get_barrier_semaphore()
    with jax.named_scope("b_signal"):
        for step_ep in range(ep_count):
            for step_tp in range(tp_count):
                if step_ep or step_tp:
                    pl.semaphore_signal(
                        barrier,
                        inc=1,
                        device_id=(
                            (ep_me + step_ep) % ep_count,
                            (tp_me + step_tp) % tp_count,
                        ),
                        device_id_type=pl.DeviceIdType.MESH,
                    )

    with jax.named_scope("c_pick"):
        row_of = lax.broadcasted_iota(jnp.int32, (rows, rows), 0)
        col_of = lax.broadcasted_iota(jnp.int32, (rows, rows), 1)

        def upright(line):
            return jnp.sum(jnp.where(row_of == col_of, line, 0.0), axis=1, keepdims=True)

        small_loads[0].wait()
        small_loads[1].wait()
        ids = ids_ref[...].astype(jnp.float32)
        mixes = mix_ref[...]
        first_id, second_id = upright(ids[0:1, :]), upright(ids[1:2, :])
        first_mix, second_mix = upright(mixes[0:1, :]), upright(mixes[1:2, :])
        group_of = jnp.zeros((rows, 1), jnp.float32)
        for chip in range(1, chips):
            group_of += (first_id >= chip * group).astype(jnp.float32)
        lanes = lax.broadcasted_iota(jnp.int32, (rows, 128), 1)
        shift = block_rows.bit_length() - 1
        earlier = (col_of < row_of) & ((col_of >> shift) == (row_of >> shift))
        member = (group_of == lanes.astype(jnp.float32)).astype(jnp.float32)
        counts = jnp.dot(
            earlier.astype(jnp.float32).astype(jnp.bfloat16),
            member.astype(jnp.bfloat16),
            preferred_element_type=jnp.float32,
        )
        rank = jnp.sum(counts * member, axis=1, keepdims=True)
        block_of = (lax.broadcasted_iota(jnp.int32, (rows, 1), 0) >> shift).astype(jnp.float32)
        target_slot = (group_of * tp_count + block_of) * cap + rank
        slots = chips * tp_count * cap
        slot_of = lax.broadcasted_iota(jnp.int32, (rows, slots), 1).astype(jnp.float32)
        pick = (slot_of == target_slot).astype(jnp.float32).astype(jnp.bfloat16)
        pick_buf[...] = pick
        across = (((0,), (0,)), ((), ()))
        small_loads[2].wait()
        send_buf[...] = lax.dot_general(
            pick, tok_ref[...], across, preferred_element_type=jnp.float32
        ).astype(jnp.bfloat16)
        in_order = first_id < second_id
        low_mix = jnp.where(in_order, first_mix, second_mix)
        high_mix = jnp.where(in_order, second_mix, first_mix)
        low_top = low_mix.astype(jnp.bfloat16).astype(jnp.float32)
        high_top = high_mix.astype(jnp.bfloat16).astype(jnp.float32)
        mix_cols = jnp.where(lanes == 0, low_top, 0.0)
        mix_cols = jnp.where(lanes == 1, high_top, mix_cols)
        mix_cols = jnp.where(lanes == 2, low_mix - low_top, mix_cols)
        mix_cols = jnp.where(lanes == 3, high_mix - high_top, mix_cols)
        weight_send[...] = lax.dot_general(
            pick, mix_cols.astype(jnp.bfloat16), across, preferred_element_type=jnp.float32
        ).astype(jnp.bfloat16)
        small_loads[3].wait()

    with jax.named_scope("d_barrier"):
        pl.semaphore_wait(barrier, ep_count * tp_count - 1)

    tail_cols = pl.ds(model_width, 128)
    with jax.named_scope("e_issue"):
        for place in (1, 0, 2, 3):
            chip = chip_me if place == 0 else entry(send_table, chip_me, place - 1)
            turn = 0 if place == 0 else turn_at(chip, chip_me)
            src = weight_send.at[slot_at(chip, tp_me)]
            dst = row_buf.at[rows_at(turn, core_me), tail_cols]
            if place == 0:
                pltpu.make_async_copy(src, dst, row_recv_sem.at[turn]).start()
            else:
                remote(
                    src,
                    dst,
                    weight_send_sem.at[0],
                    row_recv_sem.at[turn],
                    (chip * group + core_me, tp_me),
                ).start()
            for step_tp in range(tp_count):
                block = (tp_me + step_tp) % tp_count
                src = send_buf.at[slot_at(chip, block)]
                dst = row_buf.at[rows_at(turn, core_me), cols_at(tp_me)]
                if place == 0 and step_tp == 0:
                    pltpu.make_async_copy(src, dst, row_recv_sem.at[turn]).start()
                else:
                    remote(
                        src,
                        dst,
                        row_send_sem.at[0],
                        row_recv_sem.at[turn],
                        (chip * group + core_me, block),
                    ).start()
        down_copy = remote(
            down_hbm.at[0, :, half_at(core_other)],
            down_buf.at[pl.ds(hidden_width, hidden_width), :],
            down_send_sem.at[0],
            down_recv_sem.at[0],
            partner,
        )
        down_copy.start()

    def receive(turn):
        arrived = row_buf.at[rows_at(turn, core_me)]
        settle(arrived, row_recv_sem.at[turn])
        remote(
            arrived, arrived, pass_send_sem.at[0], pass_recv_sem.at[turn], partner
        ).start()

    def held_by(turns):
        return slice(min(turns) * phase_rows, (max(turns) + 1) * phase_rows)

    def widen(turns):
        held = held_by(turns)
        first = min(turns) == 0
        with jax.named_scope(f"g_passwait{min(turns)}"):
            for turn in turns:
                settle(row_buf.at[rows_at(turn, core_other)], pass_recv_sem.at[turn])
            if first:
                gate_load.wait()
                up_load.wait()
        with jax.named_scope(f"h_gate{min(turns)}"):
            widened = row_buf[held, :model_width].astype(jnp.float32)
            mean_square = jnp.mean(widened * widened, axis=-1, keepdims=True)
            normed = (widened * lax.rsqrt(mean_square + 1e-06) * gain_ref[...]).astype(
                jnp.bfloat16
            )
            both = jnp.dot(normed, wide_buf[...], preferred_element_type=jnp.float32)
            gate_part, up_part = both[:, :hidden_width], both[:, hidden_width:]
            mixes = row_buf[held, model_width:].astype(jnp.float32)
            low = mixes[:, 0:1] + mixes[:, 2:3]
            high = mixes[:, 1:2] + mixes[:, 3:4]
            mix = jnp.where(core_me == 0, low, high)
            hidden = gate_part / (1.0 + jnp.exp(-gate_part)) * up_part * mix
            hidden_buf[held, :hidden_width] = hidden.astype(jnp.bfloat16)
            remote(
                hidden_buf.at[held, :hidden_width],
                hidden_buf.at[held, hidden_width:],
                pair_send_sem.at[0],
                pair_recv_sem.at[min(turns)],
                partner,
            ).start()

    def narrow(turns):
        held = held_by(turns)
        first = min(turns) == 0
        with jax.named_scope(f"l_own{min(turns)}"):
            if first:
                down_load.wait()
            own_part = jnp.dot(
                hidden_buf[held, :hidden_width],
                down_buf[:hidden_width, :],
                preferred_element_type=jnp.float32,
            )
        with jax.named_scope(f"m_hidwait{min(turns)}"):
            settle(hidden_buf.at[held, hidden_width:], pair_recv_sem.at[min(turns)])
            if first:
                down_copy.wait_recv()
        with jax.named_scope(f"n_down{min(turns)}"):
            for part in range(half_tp):
                part_cols = slice(part * width, (part + 1) * width)
                result_buf[held, part_cols] = (
                    own_part[:, part_cols]
                    + jnp.dot(
                        hidden_buf[held, hidden_width:],
                        down_buf[hidden_width:, part_cols],
                        preferred_element_type=jnp.float32,
                    )
                ).astype(jnp.bfloat16)
                feature = core_me * half_tp + part
                for turn in turns:
                    chip = entry(turn_table, chip_me, turn)
                    for step_core in reversed(range(group)):
                        core = (core_me + step_core) % group
                        src = result_buf.at[rows_at(turn, core), part_cols]
                        dst = back_buf.at[slot_at(chip_me, tp_me)]
                        copy = remote(
                            src,
                            dst,
                            back_send_sem.at[0],
                            back_recv_sem.at[0],
                            (chip * group + core, feature),
                        )
                        if step_core == 0 and turn == 0:
                            here = feature == tp_me

                            @pl.when(here)
                            def _():
                                pltpu.make_async_copy(src, dst, back_recv_sem.at[0]).start()

                            @pl.when(jnp.logical_not(here))
                            def _():
                                copy.start()
                        else:
                            copy.start()

    inner = (chip_me + 1) // 2 % 2

    def receive_on(side, turns):
        @pl.when(inner == side)
        def _():
            for turn in turns:
                receive(turn)

    with jax.named_scope("f_recv1"):
        receive(1)
    with jax.named_scope("f_recv0"):
        receive(0)
    widen((1, 0))
    with jax.named_scope("f_recvO"):
        receive_on(0, (2, 3))
    narrow((1, 0))
    with jax.named_scope("f_recvI"):
        receive_on(1, (2, 3))
    widen((2, 3))
    narrow((2, 3))

    with jax.named_scope("o_backwait"):
        settle(back_buf, back_recv_sem.at[0])
    with jax.named_scope("p_out"):
        out_ref[...] = jnp.dot(
            pick_buf[...], back_buf[...], preferred_element_type=jnp.float32
        ).astype(out_ref.dtype)

    with jax.named_scope("q_drain"):
        settle(send_buf.at[pl.ds(0, (chips * tp_count - 1) * cap)], row_send_sem.at[0])
        settle(weight_send.at[pl.ds(0, (chips - 1) * cap)], weight_send_sem.at[0])
        settle(row_buf.at[pl.ds(0, chips * cap)], pass_send_sem.at[0])
        settle(hidden_buf.at[:, :hidden_width], pair_send_sem.at[0])
        down_copy.wait_send()
        stays = tp_me // half_tp == core_me

        @pl.when(stays)
        def _():
            settle(back_buf.at[pl.ds(0, (chips * tp_count - 1) * cap)], back_send_sem.at[0])

        @pl.when(jnp.logical_not(stays))
        def _():
            settle(back_buf, back_send_sem.at[0])


def direct(tokens, norm_gain, gate_weight, up_weight, down_weight, expert_ids, route_weight):
    ep_count, tp_count = lax.axis_size("ep"), lax.axis_size("tp")
    group = math.isqrt(ep_count * gate_weight.shape[0])
    rows, width = tokens.shape
    cap = 4 * (rows // tp_count) // ep_count * group // 2
    chips = ep_count // group
    model_width, hidden_width = gate_weight.shape[1:]
    slots = chips * tp_count * cap
    held = ep_count * cap
    half_cols = model_width // group
    vmem, dma = pltpu.VMEM, pltpu.SemaphoreType.DMA
    low = jnp.bfloat16
    in_vmem = pl.BlockSpec(memory_space=pltpu.VMEM)
    in_hbm = pl.BlockSpec(memory_space=pltpu.HBM)
    return pl.pallas_call(
        partial(direct_kernel, (ep_count, tp_count, group, cap)),
        out_shape=pltpu.VMEM((rows, width), low),
        in_specs=[in_hbm] * 7,
        out_specs=in_vmem,
        scratch_shapes=[
            vmem((2, rows), jnp.int32),
            vmem((2, rows), jnp.float32),
            vmem((rows, width), low),
            vmem((1, model_width), jnp.float32),
            vmem((rows, slots), low),
            vmem((slots, width), low),
            vmem((slots, 128), low),
            vmem((held, model_width + 128), low),
            vmem((model_width, 2 * hidden_width), low),
            vmem((2 * hidden_width, half_cols), low),
            vmem((held, 2 * hidden_width), low),
            vmem((held, half_cols), low),
            vmem((slots, width), low),
            dma((7,)),
            dma((1,)),
            dma((chips,)),
            dma((1,)),
            dma((1,)),
            dma((chips,)),
            dma((1,)),
            dma((chips,)),
            dma((1,)),
            dma((1,)),
            dma((1,)),
            dma((1,)),
        ],
        compiler_params=pltpu.CompilerParams(
            collective_id=0,
            has_side_effects=True,
            vmem_limit_bytes=67043328 - rows * width * 2,
        ),
    )(
        expert_ids.T,
        route_weight.T,
        tokens,
        norm_gain.reshape(1, -1),
        gate_weight,
        up_weight,
        down_weight,
    )


def layer(tokens, norm_gain, gate_weight, up_weight, down_weight, expert_ids, route_weight):
    group = math.isqrt(lax.axis_size("ep") * gate_weight.shape[0])
    paired = group == 2 and gate_weight.shape[0] == 1 and lax.axis_size("ep") == group**3
    body = direct if paired else local
    return body(
        tokens, norm_gain, gate_weight, up_weight, down_weight, expert_ids, route_weight
    )


def solution(mesh):
    in_specs = (
        P("ep", "tp"),
        P(),
        P("ep", None, None),
        P("ep", None, None),
        P("ep", None, None),
        P("ep", None),
        P("ep", None),
    )
    out_specs = P("ep", "tp")
    return jax.shard_map(layer, mesh=mesh, in_specs=in_specs, out_specs=out_specs, check_vma=False)
```

time: 27.1 us -> 24.3 us (0.90)
  Pallas kernels: 25.3 us -> 23.5 us
  local copies, waits for them, and re-layouts: 1.57 us -> 0.66 us
    pallas_call x1, Pallas kernels: 25.3 us -> 23.5 us  [direct(): pl.pallas_call(partial(direct_kernel, (ep_count, tp_count, group, cap)),...]
    unnamed x1, local copies, waits for them, and re-layouts: 1.57 us -> 0.66 us
where the time goes in v1:
time: 24.3 us; the launch traced here: 24.1 us
  Pallas kernels  23.5 us (97%)
  local copies, waits for them, and re-layouts  0.66 us (3%)
    pallas_call x1, Pallas kernels, direct(): pl.pallas_call(partial(direct_kernel, (ep_count, tp_count, group, cap)),...  23.5 us
    unnamed x1, local copies, waits for them, and re-layouts  0.66 us

profile of v1, /device:TPU:0, one launch (start us, length us, event | category | flops | bytes accessed | tf_op | source)
XLA Modules:
  0.0 24.1 jit_solution(15573362244260061547)
XLA Ops:
  0.0 23.5 %shard_map.73 = bf16[128,512]{1,0:T(8,128)(2,1)S(1)} custom-call(s32[2,128]{1,0:T(2,128)} %bitcast.4, f32[2,128]{1,0:T(2,128)} %bitcast.5, bf16[128,512]{1,0:T(8,128)(2,1)} %tok_hbm.1, f32[1,2048]{1,0:T(1,128)} %bitcast.3, bf16[1,2048,512]{2,1,0:T(8,128)(2,1)} %gate_hbm.1, bf16[1,2048,512]{2,1,0:T(8,128)(2,1)} %up_hbm.1, bf16[1,512,2048]{2,1,0:T(8,128)(2,1)} %down_hbm.1), custom_call_target="tpu_custom_call" | custom-call | tf_op jit(solution)/shard_map/pallas_call | solution.py:448
  23.5 0.7 %copy.9 = bf16[128,512]{1,0:T(8,128)(2,1)} copy(bf16[128,512]{1,0:T(8,128)(2,1)S(1)} %shard_map.73) | data formatting | bytes 262144

commit v2 on v1

--- a/solution.py
+++ b/solution.py
@@ -118,8 +118,9 @@
     chip_me = ep_me // group
     core_me = ep_me % group
     core_other = 1 - core_me
+    half_me = core_other
     partner = (chip_me * group + core_other, tp_me)
-    send_table = ((2, 3, 1), (3, 2, 0), (0, 1, 3), (1, 0, 2))
+    send_table = ((3, 2, 1), (3, 2, 0), (0, 1, 3), (1, 0, 2))
     turn_table = ((0, 3, 2, 1), (1, 3, 2, 0), (2, 0, 1, 3), (3, 0, 1, 2))
     phase_rows = group * cap
 
@@ -176,7 +177,7 @@
         up_hbm.at[0], wide_buf.at[:, pl.ds(hidden_width, hidden_width)], load_sem.at[1]
     )
     down_load = pltpu.make_async_copy(
-        down_hbm.at[0, :, half_at(core_me)],
+        down_hbm.at[0, :, half_at(half_me)],
         down_buf.at[pl.ds(0, hidden_width), :],
         load_sem.at[6],
     )
@@ -257,8 +258,9 @@
         for place in (1, 0, 2, 3):
             chip = chip_me if place == 0 else entry(send_table, chip_me, place - 1)
             turn = 0 if place == 0 else turn_at(chip, chip_me)
+            core = core_me if place == 0 else core_other
             src = weight_send.at[slot_at(chip, tp_me)]
-            dst = row_buf.at[rows_at(turn, core_me), tail_cols]
+            dst = row_buf.at[rows_at(turn, core), tail_cols]
             if place == 0:
                 pltpu.make_async_copy(src, dst, row_recv_sem.at[turn]).start()
             else:
@@ -267,12 +269,12 @@
                     dst,
                     weight_send_sem.at[0],
                     row_recv_sem.at[turn],
-                    (chip * group + core_me, tp_me),
+                    (chip * group + core, tp_me),
                 ).start()
             for step_tp in range(tp_count):
                 block = (tp_me + step_tp) % tp_count
                 src = send_buf.at[slot_at(chip, block)]
-                dst = row_buf.at[rows_at(turn, core_me), cols_at(tp_me)]
+                dst = row_buf.at[rows_at(turn, core), cols_at(tp_me)]
                 if place == 0 and step_tp == 0:
                     pltpu.make_async_copy(src, dst, row_recv_sem.at[turn]).start()
                 else:
@@ -281,10 +283,10 @@
                         dst,
                         row_send_sem.at[0],
                         row_recv_sem.at[turn],
-                        (chip * group + core_me, block),
+                        (chip * group + core, block),
                     ).start()
         down_copy = remote(
-            down_hbm.at[0, :, half_at(core_other)],
+            down_hbm.at[0, :, half_at(core_me)],
             down_buf.at[pl.ds(hidden_width, hidden_width), :],
             down_send_sem.at[0],
             down_recv_sem.at[0],
@@ -359,12 +361,12 @@
                         preferred_element_type=jnp.float32,
                     )
                 ).astype(jnp.bfloat16)
-                feature = core_me * half_tp + part
+                feature = half_me * half_tp + part
                 for turn in turns:
                     chip = entry(turn_table, chip_me, turn)
-                    for step_core in reversed(range(group)):
-                        core = (core_me + step_core) % group
-                        src = result_buf.at[rows_at(turn, core), part_cols]
+                    for core in range(group):
+                        held_core = core if turn == 0 else 1 - core
+                        src = result_buf.at[rows_at(turn, held_core), part_cols]
                         dst = back_buf.at[slot_at(chip_me, tp_me)]
                         copy = remote(
                             src,
@@ -373,8 +375,8 @@
                             back_recv_sem.at[0],
                             (chip * group + core, feature),
                         )
-                        if step_core == 0 and turn == 0:
-                            here = feature == tp_me
+                        if turn == 0:
+                            here = (feature == tp_me) & (core == core_me)
 
                             @pl.when(here)
                             def _():
@@ -420,7 +422,7 @@
         settle(row_buf.at[pl.ds(0, chips * cap)], pass_send_sem.at[0])
         settle(hidden_buf.at[:, :hidden_width], pair_send_sem.at[0])
         down_copy.wait_send()
-        stays = tp_me // half_tp == core_me
+        stays = tp_me // half_tp == half_me
 
         @pl.when(stays)
         def _():

time: 24.3 us -> 23.6 us (0.971)
  Pallas kernels: 23.5 us -> 22.6 us
    pallas_call x1, Pallas kernels: 23.5 us -> 22.6 us  [direct(): pl.pallas_call(partial(direct_kernel, (ep_count, tp_count, group, cap)),...]
where the time goes in v2:
time: 23.6 us; the launch traced here: 23.3 us
  Pallas kernels  22.6 us (96%)
  local copies, waits for them, and re-layouts  0.66 us (3%)
    pallas_call x1, Pallas kernels, direct(): pl.pallas_call(partial(direct_kernel, (ep_count, tp_count, group, cap)),...  22.6 us
    unnamed x1, local copies, waits for them, and re-layouts  0.66 us

profile of v2, /device:TPU:0, one launch (start us, length us, event | category | flops | bytes accessed | tf_op | source)
XLA Modules:
  0.0 23.3 jit_solution(12586467916679879838)
XLA Ops:
  0.0 22.6 %shard_map.73 = bf16[128,512]{1,0:T(8,128)(2,1)S(1)} custom-call(s32[2,128]{1,0:T(2,128)} %bitcast.4, f32[2,128]{1,0:T(2,128)} %bitcast.5, bf16[128,512]{1,0:T(8,128)(2,1)} %tok_hbm.1, f32[1,2048]{1,0:T(1,128)} %bitcast.3, bf16[1,2048,512]{2,1,0:T(8,128)(2,1)} %gate_hbm.1, bf16[1,2048,512]{2,1,0:T(8,128)(2,1)} %up_hbm.1, bf16[1,512,2048]{2,1,0:T(8,128)(2,1)} %down_hbm.1), custom_call_target="tpu_custom_call" | custom-call | tf_op jit(solution)/shard_map/pallas_call | solution.py:450
  22.6 0.7 %copy.9 = bf16[128,512]{1,0:T(8,128)(2,1)} copy(bf16[128,512]{1,0:T(8,128)(2,1)S(1)} %shard_map.73) | data formatting | bytes 262144

commit v3 on v2

--- a/solution.py
+++ b/solution.py
@@ -87,6 +87,7 @@
     send_buf,
     weight_send,
     row_buf,
+    normed_buf,
     wide_buf,
     down_buf,
     hidden_buf,
@@ -138,6 +139,12 @@
         for late in range(1, chips):
             turn = jnp.where(entry(turn_table, here, late) == there, late, turn)
         return turn
+
+    def across_tp(step):
+        block, bit = 0, 1
+        while bit < tp_count:
+            block, bit = block + (tp_me // bit + step // bit) % 2 * bit, 2 * bit
+        return block
 
     def rows_at(turn, core):
         return pl.ds(pl.multiple_of((turn * group + core) * cap, cap), cap)
@@ -259,6 +266,20 @@
             chip = chip_me if place == 0 else entry(send_table, chip_me, place - 1)
             turn = 0 if place == 0 else turn_at(chip, chip_me)
             core = core_me if place == 0 else core_other
+            for step_tp in (3, 2, 1, 0):
+                block = across_tp(step_tp)
+                src = send_buf.at[slot_at(chip, block)]
+                dst = row_buf.at[rows_at(turn, core), cols_at(tp_me)]
+                if place == 0 and step_tp == 0:
+                    pltpu.make_async_copy(src, dst, row_recv_sem.at[turn]).start()
+                else:
+                    remote(
+                        src,
+                        dst,
+                        row_send_sem.at[0],
+                        row_recv_sem.at[turn],
+                        (chip * group + core, block),
+                    ).start()
             src = weight_send.at[slot_at(chip, tp_me)]
             dst = row_buf.at[rows_at(turn, core), tail_cols]
             if place == 0:
@@ -271,20 +292,6 @@
                     row_recv_sem.at[turn],
                     (chip * group + core, tp_me),
                 ).start()
-            for step_tp in range(tp_count):
-                block = (tp_me + step_tp) % tp_count
-                src = send_buf.at[slot_at(chip, block)]
-                dst = row_buf.at[rows_at(turn, core), cols_at(tp_me)]
-                if place == 0 and step_tp == 0:
-                    pltpu.make_async_copy(src, dst, row_recv_sem.at[turn]).start()
-                else:
-                    remote(
-                        src,
-                        dst,
-                        row_send_sem.at[0],
-                        row_recv_sem.at[turn],
-                        (chip * group + core, block),
-                    ).start()
         down_copy = remote(
             down_hbm.at[0, :, half_at(core_me)],
             down_buf.at[pl.ds(hidden_width, hidden_width), :],
@@ -304,9 +311,20 @@
     def held_by(turns):
         return slice(min(turns) * phase_rows, (max(turns) + 1) * phase_rows)
 
+    def normalize(turns, core):
+        for turn in turns:
+            picked = rows_at(turn, core)
+            widened = row_buf[picked, :model_width].astype(jnp.float32)
+            mean_square = jnp.mean(widened * widened, axis=-1, keepdims=True)
+            normed_buf[picked, :] = (
+                widened * lax.rsqrt(mean_square + 1e-06) * gain_ref[...]
+            ).astype(jnp.bfloat16)
+
     def widen(turns):
         held = held_by(turns)
         first = min(turns) == 0
+        with jax.named_scope(f"g_own{min(turns)}"):
+            normalize(turns, core_me)
         with jax.named_scope(f"g_passwait{min(turns)}"):
             for turn in turns:
                 settle(row_buf.at[rows_at(turn, core_other)], pass_recv_sem.at[turn])
@@ -314,12 +332,8 @@
                 gate_load.wait()
                 up_load.wait()
         with jax.named_scope(f"h_gate{min(turns)}"):
-            widened = row_buf[held, :model_width].astype(jnp.float32)
-            mean_square = jnp.mean(widened * widened, axis=-1, keepdims=True)
-            normed = (widened * lax.rsqrt(mean_square + 1e-06) * gain_ref[...]).astype(
-                jnp.bfloat16
-            )
-            both = jnp.dot(normed, wide_buf[...], preferred_element_type=jnp.float32)
+            normalize(turns, core_other)
+            both = jnp.dot(normed_buf[held, :], wide_buf[...], preferred_element_type=jnp.float32)
             gate_part, up_part = both[:, :hidden_width], both[:, hidden_width:]
             mixes = row_buf[held, model_width:].astype(jnp.float32)
             low = mixes[:, 0:1] + mixes[:, 2:3]
@@ -461,6 +475,7 @@
             vmem((slots, width), low),
             vmem((slots, 128), low),
             vmem((held, model_width + 128), low),
+            vmem((held, model_width), low),
             vmem((model_width, 2 * hidden_width), low),
             vmem((2 * hidden_width, half_cols), low),
             vmem((held, 2 * hidden_width), low),

time: 23.6 us -> 22.7 us (0.962)
  Pallas kernels: 22.6 us -> 21.9 us
    pallas_call x1, Pallas kernels: 22.6 us -> 21.9 us  [direct(): pl.pallas_call(partial(direct_kernel, (ep_count, tp_count, group, cap)),...]
where the time goes in v3:
time: 22.7 us; the launch traced here: 22.5 us
  Pallas kernels  21.9 us (96%)
  local copies, waits for them, and re-layouts  0.66 us (3%)
    pallas_call x1, Pallas kernels, direct(): pl.pallas_call(partial(direct_kernel, (ep_count, tp_count, group, cap)),...  21.9 us
    unnamed x1, local copies, waits for them, and re-layouts  0.66 us

profile of v3, /device:TPU:0, one launch (start us, length us, event | category | flops | bytes accessed | tf_op | source)
XLA Modules:
  0.0 22.5 jit_solution(13821331603627043277)
XLA Ops:
  0.0 21.9 %shard_map.73 = bf16[128,512]{1,0:T(8,128)(2,1)S(1)} custom-call(s32[2,128]{1,0:T(2,128)} %bitcast.4, f32[2,128]{1,0:T(2,128)} %bitcast.5, bf16[128,512]{1,0:T(8,128)(2,1)} %tok_hbm.1, f32[1,2048]{1,0:T(1,128)} %bitcast.3, bf16[1,2048,512]{2,1,0:T(8,128)(2,1)} %gate_hbm.1, bf16[1,2048,512]{2,1,0:T(8,128)(2,1)} %up_hbm.1, bf16[1,512,2048]{2,1,0:T(8,128)(2,1)} %down_hbm.1), custom_call_target="tpu_custom_call" | custom-call | tf_op jit(solution)/shard_map/pallas_call | solution.py:464
  21.9 0.7 %copy.9 = bf16[128,512]{1,0:T(8,128)(2,1)} copy(bf16[128,512]{1,0:T(8,128)(2,1)S(1)} %shard_map.73) | data formatting | bytes 262144

commit v4 on v3

--- a/solution.py
+++ b/solution.py
@@ -122,7 +122,7 @@
     half_me = core_other
     partner = (chip_me * group + core_other, tp_me)
     send_table = ((3, 2, 1), (3, 2, 0), (0, 1, 3), (1, 0, 2))
-    turn_table = ((0, 3, 2, 1), (1, 3, 2, 0), (2, 0, 1, 3), (3, 0, 1, 2))
+    turn_table = ((0, 3, 2, 1), (1, 3, 0, 2), (2, 0, 1, 3), (3, 0, 1, 2))
     phase_rows = group * cap
 
     def slot_at(chip, block):
@@ -410,10 +410,10 @@
             for turn in turns:
                 receive(turn)
 
+    with jax.named_scope("f_recv0"):
+        receive(0)
     with jax.named_scope("f_recv1"):
         receive(1)
-    with jax.named_scope("f_recv0"):
-        receive(0)
     widen((1, 0))
     with jax.named_scope("f_recvO"):
         receive_on(0, (2, 3))

time: 22.7 us -> 22.6 us (level)
  no operation moved by 1% of the time
where the time goes in v4:
time: 22.6 us; the launch traced here: 22.4 us
  Pallas kernels  21.8 us (96%)
  local copies, waits for them, and re-layouts  0.66 us (3%)
    pallas_call x1, Pallas kernels, direct(): pl.pallas_call(partial(direct_kernel, (ep_count, tp_count, group, cap)),...  21.8 us
    unnamed x1, local copies, waits for them, and re-layouts  0.66 us

profile of v4, /device:TPU:0, one launch (start us, length us, event | category | flops | bytes accessed | tf_op | source)
XLA Modules:
  0.0 22.4 jit_solution(12339228488250972541)
XLA Ops:
  0.0 21.8 %shard_map.73 = bf16[128,512]{1,0:T(8,128)(2,1)S(1)} custom-call(s32[2,128]{1,0:T(2,128)} %bitcast.4, f32[2,128]{1,0:T(2,128)} %bitcast.5, bf16[128,512]{1,0:T(8,128)(2,1)} %tok_hbm.1, f32[1,2048]{1,0:T(1,128)} %bitcast.3, bf16[1,2048,512]{2,1,0:T(8,128)(2,1)} %gate_hbm.1, bf16[1,2048,512]{2,1,0:T(8,128)(2,1)} %up_hbm.1, bf16[1,512,2048]{2,1,0:T(8,128)(2,1)} %down_hbm.1), custom_call_target="tpu_custom_call" | custom-call | tf_op jit(solution)/shard_map/pallas_call | solution.py:464
  21.8 0.7 %copy.9 = bf16[128,512]{1,0:T(8,128)(2,1)} copy(bf16[128,512]{1,0:T(8,128)(2,1)S(1)} %shard_map.73) | data formatting | bytes 262144

commit v5 on v4

--- a/solution.py
+++ b/solution.py
@@ -181,19 +181,19 @@
         gate_hbm.at[0], wide_buf.at[:, pl.ds(0, hidden_width)], load_sem.at[0]
     )
     up_load = pltpu.make_async_copy(
-        up_hbm.at[0], wide_buf.at[:, pl.ds(hidden_width, hidden_width)], load_sem.at[1]
+        up_hbm.at[0], wide_buf.at[:, pl.ds(hidden_width, hidden_width)], load_sem.at[0]
     )
     down_load = pltpu.make_async_copy(
         down_hbm.at[0, :, half_at(half_me)],
         down_buf.at[pl.ds(0, hidden_width), :],
-        load_sem.at[6],
+        load_sem.at[1],
     )
     for load in small_loads + [gate_load, up_load, down_load]:
         load.start()
 
     barrier = pltpu.get_barrier_semaphore()
     with jax.named_scope("b_signal"):
-        for step_ep in range(ep_count):
+        for step_ep in (*range(1, ep_count), 0):
             for step_tp in range(tp_count):
                 if step_ep or step_tp:
                     pl.semaphore_signal(
@@ -329,8 +329,7 @@
             for turn in turns:
                 settle(row_buf.at[rows_at(turn, core_other)], pass_recv_sem.at[turn])
             if first:
-                gate_load.wait()
-                up_load.wait()
+                settle(wide_buf, load_sem.at[0])
         with jax.named_scope(f"h_gate{min(turns)}"):
             normalize(turns, core_other)
             both = jnp.dot(normed_buf[held, :], wide_buf[...], preferred_element_type=jnp.float32)
@@ -481,7 +480,7 @@
             vmem((held, 2 * hidden_width), low),
             vmem((held, half_cols), low),
             vmem((slots, width), low),
-            dma((7,)),
+            dma((6,)),
             dma((1,)),
             dma((chips,)),
             dma((1,)),

time: 22.6 us -> 22.6 us (level)
  no operation moved by 1% of the time
where the time goes in v5:
time: 22.6 us; the launch traced here: 22.4 us
  Pallas kernels  21.7 us (96%)
  local copies, waits for them, and re-layouts  0.66 us (3%)
    pallas_call x1, Pallas kernels, direct(): pl.pallas_call(partial(direct_kernel, (ep_count, tp_count, group, cap)),...  21.7 us
    unnamed x1, local copies, waits for them, and re-layouts  0.66 us

profile of v5, /device:TPU:0, one launch (start us, length us, event | category | flops | bytes accessed | tf_op | source)
XLA Modules:
  0.0 22.4 jit_solution(6901331583855514877)
XLA Ops:
  0.0 21.7 %shard_map.73 = bf16[128,512]{1,0:T(8,128)(2,1)S(1)} custom-call(s32[2,128]{1,0:T(2,128)} %bitcast.4, f32[2,128]{1,0:T(2,128)} %bitcast.5, bf16[128,512]{1,0:T(8,128)(2,1)} %tok_hbm.1, f32[1,2048]{1,0:T(1,128)} %bitcast.3, bf16[1,2048,512]{2,1,0:T(8,128)(2,1)} %gate_hbm.1, bf16[1,2048,512]{2,1,0:T(8,128)(2,1)} %up_hbm.1, bf16[1,512,2048]{2,1,0:T(8,128)(2,1)} %down_hbm.1), custom_call_target="tpu_custom_call" | custom-call | tf_op jit(solution)/shard_map/pallas_call | solution.py:463
  21.7 0.7 %copy.9 = bf16[128,512]{1,0:T(8,128)(2,1)} copy(bf16[128,512]{1,0:T(8,128)(2,1)S(1)} %shard_map.73) | data formatting | bytes 262144
